TPU v7x, 32 devices: a whole 2x2x4 slice. The times are simulated.
32 devices in a mesh: ep: 8 (over z, y), tp: 4 (over x, core).
Axes of the slice: x: 2, y: 2, z: 4, core: 2. Of those that a mesh axis runs over, the one named last changes fastest.
Arguments:
- tokens: bfloat16 [256, 2048], P('ep', 'tp'), may hold values from -33 to 33
- previous: bfloat16 [256, 2048], P('ep', 'tp'), may hold values from -6 to 6
- first_norm_gain: float32 [2048], replicated, may hold values from 0.1 to 1.9
- token_shift_share: float32 [5, 2048], replicated, may hold values from 0 to 1
- receptance_weight: bfloat16 [2048, 1024], P(None, 'tp'), may hold values from -0.125 to 0.125
- key_weight: bfloat16 [2048, 1024], P(None, 'tp'), may hold values from -0.125 to 0.125
- value_weight: bfloat16 [2048, 1024], P(None, 'tp'), may hold values from -0.125 to 0.125
- decay_down_map: bfloat16 [2048, 128], replicated, may hold values from -0.125 to 0.125
- decay_up_map: bfloat16 [128, 1024], replicated, may hold values from -0.5 to 0.5
- decay_offset: float32 [1024], P('tp'), may hold values from -4 to 1
- strength_down_map: bfloat16 [2048, 128], replicated, may hold values from -0.125 to 0.125
- strength_up_map: bfloat16 [128, 1024], replicated, may hold values from -0.5 to 0.5
- removal_key_scale: float32 [1024], P('tp'), may hold values from 0.3 to 3
- key_damping: float32 [1024], P('tp'), may hold values from 0.1 to 1.9
- self_term_weight: float32 [16, 64], P('tp'), may hold values from -0.6 to 0.6
- head_norm_gain: float32 [1024], P('tp'), may hold values from 0.1 to 1.9
- output_weight: bfloat16 [1024, 2048], P('tp'), may hold values from -0.1875 to 0.1875
- state: float32 [256, 16, 64, 64], P('ep', 'tp'), may hold values from -6 to 6
- second_norm_gain: float32 [2048], replicated, may hold values from 0.1 to 1.9
- routes: int32 [256, 4], P('ep'), may hold values from 0 to 7, all different within a row; in each aligned block of 32 rows (0 to 31, 32 to 63, ...) at most 24 rows name the same one
- chosen_expert_weight: float32 [256, 4], P('ep'), may hold values from 0.1 to 1
- expert_gate_weight: bfloat16 [8, 2048, 1024], P('ep', None, 'tp'), may hold values from -0.5 to 0.5
- expert_up_weight: bfloat16 [8, 2048, 1024], P('ep', None, 'tp'), may hold values from -0.5 to 0.5
- expert_down_weight: bfloat16 [8, 1024, 2048], P('ep', 'tp'), may hold values from -0.046875 to 0.046875
Outputs:
- layer_out: bfloat16 [256, 2048], P('ep', 'tp')
- new_state: float32 [256, 16, 64, 64], P('ep', 'tp')
Inputs may be any that keep to these rules, and one draw needn't show every extreme that they name: `routes`: each row names 4 different experts. Among the rows of one index of ep no expert is named by more than 24 rows, and in every draw some expert is named by exactly 24 rows of some index of ep.
All inputs are finite; a program needn't handle non-finite values.
Results may differ from a plain program's by a relative error of at most 0.015.
Values may be sent and summed in bfloat16 or wider, within the bound.
A program may use at most 64 MiB of HBM per device.

v0:
```python
import jax
import jax.numpy as jnp
from jax import lax
from jax.sharding import PartitionSpec as P

NORM_EPS = 1e-06
GROUP_EPS = 0.00064
KEY_EPS = 1e-06
GATE_LIMIT = 7.0
GATE_SLOPE = 1.702


def row_rescale(values, gain):
    return values * lax.rsqrt(jnp.mean(values * values, axis=-1, keepdims=True) + NORM_EPS) * gain


def head_combiner(
    present_rows,
    prior_rows,
    first_norm_gain,
    token_shift_share,
    receptance_weight,
    key_weight,
    value_weight,
    decay_down_map,
    decay_up_map,
    decay_offset,
    strength_down_map,
    strength_up_map,
    removal_key_scale,
    key_damping,
    self_term_weight,
    head_norm_gain,
    state,
):
    sequence_count = present_rows.shape[0]
    head_number = state.shape[1]
    head_extent = state.shape[2]
    normed = row_rescale(present_rows.astype(jnp.float32), first_norm_gain)
    before = prior_rows.astype(jnp.float32)

    def shifted(role):
        return (normed + (before - normed) * token_shift_share[role]).astype(jnp.bfloat16)

    def project(inputs, weight):
        return jnp.dot(inputs, weight, preferred_element_type=jnp.float32)

    def by_heads(values):
        return values.reshape(sequence_count, head_number, head_extent)

    receptance_rows = by_heads(project(shifted(0), receptance_weight))
    key_rows = by_heads(project(shifted(1), key_weight))
    value_matrix = by_heads(project(shifted(2), value_weight))
    decay_low = jnp.tanh(project(shifted(3), decay_down_map)).astype(jnp.bfloat16)
    decay_pre = decay_offset + project(decay_low, decay_up_map)
    decay = by_heads(jnp.exp(-jnp.exp(-jax.nn.softplus(-decay_pre) - 0.5)))
    alpha_low = project(shifted(4), strength_down_map).astype(jnp.bfloat16)
    alpha = by_heads(jax.nn.sigmoid(project(alpha_low, strength_up_map)))
    removal = key_rows * removal_key_scale.reshape(head_number, head_extent)
    removal = removal * lax.rsqrt(jnp.sum(removal * removal, axis=-1, keepdims=True) + KEY_EPS)
    blended_rows = key_rows * (1.0 + (alpha - 1.0) * key_damping.reshape(head_number, head_extent))
    highest = lax.Precision.HIGHEST
    along = jnp.einsum("shij,shj->shi", state, removal, precision=highest)
    new_state = (
        state * decay[:, :, None, :]
        - along[..., None] * (removal * alpha)[:, :, None, :]
        + value_matrix[..., None] * blended_rows[:, :, None, :]
    )
    readout = jnp.einsum("shij,shj->shi", new_state, receptance_rows, precision=highest)
    centered = readout - jnp.mean(readout, axis=-1, keepdims=True)
    variance = jnp.mean(centered * centered, axis=-1, keepdims=True)
    heads_normalised = (
        centered
        * lax.rsqrt(variance + GROUP_EPS)
        * head_norm_gain.reshape(head_number, head_extent)
    )
    self_term = (
        jnp.sum(receptance_rows * blended_rows * self_term_weight, axis=-1, keepdims=True)
        * value_matrix
    )
    mixed_inputs = (
        (heads_normalised + self_term)
        .reshape(sequence_count, head_number * head_extent)
        .astype(jnp.bfloat16)
    )
    return (mixed_inputs, new_state)


def shards(
    tokens,
    previous,
    first_norm_gain,
    token_shift_share,
    receptance_weight,
    key_weight,
    value_weight,
    decay_down_map,
    decay_up_map,
    decay_offset,
    strength_down_map,
    strength_up_map,
    removal_key_scale,
    key_damping,
    self_term_weight,
    head_norm_gain,
    output_weight,
    state,
    second_norm_gain,
    routes,
    chosen_expert_weight,
    expert_gate_weight,
    expert_up_weight,
    expert_down_weight,
):
    present_rows, prior_rows = (
        lax.all_gather(tokens, "tp", axis=1, tiled=True),
        lax.all_gather(previous, "tp", axis=1, tiled=True),
    )
    head_columns = receptance_weight.shape[1]
    head_start = lax.axis_index("tp") * head_columns
    decay_own = lax.dynamic_slice_in_dim(decay_up_map, head_start, head_columns, 1)
    alpha_own = lax.dynamic_slice_in_dim(strength_up_map, head_start, head_columns, 1)
    mixed_inputs, new_state = head_combiner(
        present_rows,
        prior_rows,
        first_norm_gain,
        token_shift_share,
        receptance_weight,
        key_weight,
        value_weight,
        decay_down_map,
        decay_own,
        decay_offset,
        strength_down_map,
        alpha_own,
        removal_key_scale,
        key_damping,
        self_term_weight,
        head_norm_gain,
        state,
    )
    head_terms = jnp.dot(mixed_inputs, output_weight, preferred_element_type=jnp.float32)
    own_columns = tokens.shape[1]
    column_start = lax.axis_index("tp") * own_columns
    residual = present_rows.astype(jnp.float32) + lax.psum(
        head_terms.astype(jnp.bfloat16), "tp"
    ).astype(jnp.float32)
    expert_rows = row_rescale(residual, second_norm_gain).astype(jnp.bfloat16)
    residual_own = lax.dynamic_slice_in_dim(residual, column_start, own_columns, 1)
    normed_own = lax.dynamic_slice_in_dim(expert_rows, column_start, own_columns, 1)
    sequences, choices_per = routes.shape
    experts = expert_gate_weight.shape[0] * lax.axis_size("ep")
    capacity = max(2, 3 * sequences * choices_per // (2 * experts))
    flattened = routes.reshape(-1)
    onehot = (flattened[:, None] == jnp.arange(experts, dtype=jnp.int32)[None, :]).astype(jnp.int32)
    ranking = jnp.sum((jnp.cumsum(onehot, axis=0) - onehot) * onehot, axis=1)
    slot_index = flattened * capacity + ranking
    placing = jnp.arange(experts * capacity, dtype=jnp.int32)[:, None] == slot_index[None, :]
    dispatch = jnp.sum(
        placing.reshape(experts * capacity, sequences, choices_per).astype(jnp.int32), axis=2
    ).astype(jnp.bfloat16)
    outgoing = jnp.dot(dispatch, normed_own, preferred_element_type=jnp.float32).astype(
        jnp.bfloat16
    )
    outgoing = outgoing.reshape(experts, capacity, -1)
    arrived = lax.all_gather(
        lax.all_to_all(outgoing, "ep", split_axis=0, concat_axis=0, tiled=True),
        "tp",
        axis=2,
        tiled=True,
    )
    sources, slot_count, feature_count = arrived.shape
    expert_input = arrived.reshape(sources * slot_count, feature_count)
    gate_pre = jnp.minimum(
        jnp.dot(expert_input, expert_gate_weight[0], preferred_element_type=jnp.float32), GATE_LIMIT
    )
    up_pre = jnp.clip(
        jnp.dot(expert_input, expert_up_weight[0], preferred_element_type=jnp.float32),
        -GATE_LIMIT,
        GATE_LIMIT,
    )
    activation = ((up_pre + 1.0) * gate_pre * jax.nn.sigmoid(GATE_SLOPE * gate_pre)).astype(
        jnp.bfloat16
    )
    down_terms = jnp.dot(activation, expert_down_weight[0], preferred_element_type=jnp.float32)
    down_terms = down_terms.reshape(sources, slot_count, -1)
    shares = lax.psum_scatter(
        down_terms.astype(jnp.bfloat16), "tp", scatter_dimension=2, tiled=True
    )
    returned = lax.all_to_all(shares, "ep", split_axis=0, concat_axis=0, tiled=True)
    returned_rows = returned.reshape(experts * capacity, -1)
    picked = jnp.take(returned_rows, slot_index, axis=0).astype(jnp.float32)
    weighted = jnp.sum(
        picked.reshape(sequences, choices_per, -1) * chosen_expert_weight[:, :, None], axis=1
    )
    layer_out = (residual_own + weighted).astype(jnp.bfloat16)
    return (layer_out, new_state)


def solution(mesh):
    in_specs = (
        P("ep", "tp"),
        P("ep", "tp"),
        P(),
        P(),
        P(None, "tp"),
        P(None, "tp"),
        P(None, "tp"),
        P(),
        P(),
        P("tp"),
        P(),
        P(),
        P("tp"),
        P("tp"),
        P("tp", None),
        P("tp"),
        P("tp", None),
        P("ep", "tp", None, None),
        P(),
        P("ep", None),
        P("ep", None),
        P("ep", None, "tp"),
        P("ep", None, "tp"),
        P("ep", "tp", None),
    )
    out_specs = (P("ep", "tp"), P("ep", "tp", None, None))
    return jax.shard_map(shards, mesh=mesh, in_specs=in_specs, out_specs=out_specs, check_vma=False)
```

profile of v0, /device:TPU:0, one launch (start us, length us, event | category | flops | bytes accessed | tf_op | source)
XLA Modules:
  0.0 153.4 jit_solution(18078987325772897809)
XLA Ops:
  7.3 6.9 %all_gather.9 = bf16[32,2048]{1,0:T(8,128)(2,1)S(1)} all-gather(bf16[32,512]{1,0:T(8,128)(2,1)} %param.24), channel_id=1, replica_groups=mesh['ep'=8,'tp'=4] {'tp'}, dimensions={1}, use_global_device_ids=true | all-gather | bytes 163840 | tf_op jit(solution)/shard_map/all_gather | solution.py:116
  14.1 0.1 fusion.16
  14.3 5.8 %all_gather.10 = bf16[32,2048]{1,0:T(8,128)(2,1)S(1)} all-gather(bf16[32,512]{1,0:T(8,128)(2,1)} %param.25), channel_id=1, replica_groups=mesh['ep'=8,'tp'=4] {'tp'}, dimensions={1}, use_global_device_ids=true | all-gather | bytes 163840 | tf_op jit(solution)/shard_map/all_gather | solution.py:117
  20.1 1.1 fusion.83
  21.2 1.6 %fusion.29 = f32[32,256]{1,0:T(8,128)S(1)} fusion(bf16[2048,256]{1,0:T(8,128)(2,1)} %param.28, bf16[32,2048]{1,0:T(8,128)(2,1)S(1)} %all_gather.9, bf16[32,2048]{1,0:T(8,128)(2,1)S(1)} %all_gather.10, f32[2048]{0:T(1024)S(1)} %bitcast.60, f32[2048]{0:T(1024)} %param.26, f32[32]{0:T(128)S(1)} %add_rsqrt_fusion.3), kind=kOutput, calls=%fused_computation.45 | convolution fusion | flops 34078720 | bytes 1360000 | tf_op jit(solution)/shard_map/dot_general | solution.py:46
  22.7 0.1 reshape.176
  22.8 0.7 reshape.161
  23.5 1.4 fusion.10
  25.0 0.1 reshape.160
  25.1 1.6 %fusion.35 = f32[32,256]{1,0:T(8,128)S(1)} fusion(bf16[2048,256]{1,0:T(8,128)(2,1)} %param.29, bf16[32,2048]{1,0:T(8,128)(2,1)S(1)} %all_gather.9, bf16[32,2048]{1,0:T(8,128)(2,1)S(1)} %all_gather.10, f32[2048]{0:T(1024)S(1)} %bitcast.59, f32[2048]{0:T(1024)} %param.26, f32[32]{0:T(128)S(1)} %add_rsqrt_fusion.3), kind=kOutput, calls=%fused_computation.47 | convolution fusion | flops 34078720 | bytes 1360000 | tf_op jit(solution)/shard_map/dot_general | solution.py:46
  26.6 0.1 reshape.159
  26.8 0.1 multiply_reduce_fusion.3
  27.1 1.3 fusion.67
  28.3 0.1 mul.284
  28.5 0.3 fusion.31
  28.8 0.1 mul.306
  28.9 0.1 fusion.82
  29.0 8.5 %fusion.84 = f32[32,4,1,64]{3,2,1,0:T(1,128)S(1)} fusion(f32[32,4,64,1]{2,3,1,0:T(1,128)S(1)} %bitcast.56, f32[32,4,64,64]{3,2,1,0:T(8,128)} %param.41), kind=kOutput, calls=%fused_computation.105 | convolution fusion | flops 6291456 | bytes 2162688 | tf_op jit(solution)/shard_map/shij,shj->shi/dot_general | solution.py:63
  37.5 2.8 %multiply_add_fusion = f32[32,4,64,64]{3,2,1,0:T(8,128)S(1)} fusion(f32[32,4,64,64]{3,2,1,0:T(8,128)S(1)} %copy-done.1, f32[32,4,64]{2,1,0:T(4,128)S(1)} %get-tuple-element.8, f32[32,4,64]{2,1,0:T(4,128)S(1)} %mul.306, f32[32,4,64]{2,1,0:T(4,128)S(1)} %get-tuple-element.4, f32[32,4,64]{2,1,0:T(4,128)S(1)} %bitcast.54, f32[32,4,64]{2,1,0:T(4,128)S(1)} %mul.284), kind=kLoop, calls=%fused_computation.2 | loop fusion | flops 2621440 | bytes 4358144 | tf_op jit(solution)/shard_map/add | solution.py:65
  40.4 2.0 %copy-done.2 = f32[32,4,64,64]{3,2,1,0:T(8,128)} copy-done((f32[32,4,64,64]{3,2,1,0:T(8,128)}, f32[32,4,64,64]{3,2,1,0:T(8,128)S(1)}, u32[]{:S(2)}) %copy-start.2) | copy-done | bytes 2097176
  42.3 6.6 %fusion.85 = f32[32,4,1,64]{3,2,1,0:T(1,128)S(1)} fusion(f32[32,4,64,64]{3,2,1,0:T(8,128)S(1)} %multiply_add_fusion, f32[32,4,64,1]{2,3,1,0:T(1,128)S(1)} %bitcast.55), kind=kOutput, calls=%fused_computation.106 | convolution fusion | flops 6291456 | bytes 2162688 | tf_op jit(solution)/shard_map/shij,shj->shi/dot_general | solution.py:69
  48.9 0.1 reduce_sum.87
  49.1 0.2 multiply_reduce_fusion.2
  49.2 0.6 add_rsqrt_fusion
  49.9 1.4 fusion.7
  51.3 0.1 convert_element_type.78
  51.4 0.9 convolution_convert_fusion.1
  52.5 0.1 reshape.162
  52.7 0.2 reduce_window_sum.11
  52.9 0.2 select_reduce_fusion
  53.1 0.1 reduce_sum.91
  53.3 0.8 dynamic-slice
  54.2 31.7 %all-reduce.2.cloned.1.call-done = bf16[32,2048]{1,0:T(8,128)(2,1)} async-done(((bf16[32,2048]{1,0:T(8,128)(2,1)}), bf16[32,2048]{1,0:T(8,128)(2,1)}) %all-reduce.2.cloned.1.call-update) | async-done | bytes 131088 | tf_op jit(solution)/shard_map/psum | solution.py:145
  85.8 1.1 multiply_reduce_fusion.1
  87.0 0.3 convolution_convert_fusion.2
  87.3 13.1 %all_to_all.10 = bf16[8,24,512]{2,1,0:T(8,128)(2,1)S(1)} all-to-all(bf16[8,24,512]{2,1,0:T(8,128)(2,1)S(1)} %bitcast.50), channel_id=1, replica_groups=mesh['ep'=8,'tp'=4] {'ep'}, dimensions={0} | all-to-all | bytes 393216 | tf_op jit(solution)/shard_map/all_to_all | solution.py:167
  100.3 7.6 %all_gather.11 = bf16[8,24,2048]{2,1,0:T(8,128)(2,1)S(1)} all-gather(bf16[8,24,512]{2,1,0:T(8,128)(2,1)S(1)} %all_to_all.10), channel_id=1, replica_groups=mesh['ep'=8,'tp'=4] {'tp'}, dimensions={2}, use_global_device_ids=true | all-gather | bytes 983040 | tf_op jit(solution)/shard_map/all_gather | solution.py:166
  107.9 0.4 convolution_minimum_fusion
  108.3 0.4 fusion.4
  108.7 1.3 convolution_convert_fusion
  110.0 21.4 %reduce-scatter.2.cloned.1.call-done = bf16[8,24,512]{2,1,0:T(8,128)(2,1)} async-done(((bf16[8,24,2048]{2,1,0:T(8,128)(2,1)}), bf16[8,24,512]{2,1,0:T(8,128)(2,1)}) %reduce-scatter.2.cloned.1.call-update) | async-done | bytes 196624 | tf_op jit(solution)/shard_map/reduce_scatter | solution.py:187
  131.5 5.5 %all-to-all-start.1 = ((bf16[8,24,512]{2,1,0:T(8,128)(2,1)}), bf16[8,24,512]{2,1,0:T(8,128)(2,1)S(1)}, u32[]{:S(2)}, u32[]{:S(2)}) async-start(bf16[8,24,512]{2,1,0:T(8,128)(2,1)} %reduce-scatter.2.cloned.1.call-done), calls=%async_computation.2 | async-start | bytes 393216 | tf_op jit(solution)/shard_map/all_to_all | solution.py:190
  137.1 0.1 mul.341
  137.2 0.1 copy.38
  137.4 7.4 %all-to-all-done.1 = bf16[8,24,512]{2,1,0:T(8,128)(2,1)S(1)} async-done(((bf16[8,24,512]{2,1,0:T(8,128)(2,1)}), bf16[8,24,512]{2,1,0:T(8,128)(2,1)S(1)}, u32[]{:S(2)}, u32[]{:S(2)}) %all-to-all-start.1) | async-done | bytes 196640 | tf_op jit(solution)/shard_map/all_to_all | solution.py:190
  144.8 0.8 gather_fusion
  145.7 0.3 multiply_reduce_fusion
  145.9 0.6 add_convert_fusion
  (53 shorter events, 1.0 us)
Async XLA Ops:
  7.2 101.6 %copy-start = (bf16[1,256,2048]{2,1,0:T(8,128)(2,1)S(1)}, bf16[1,256,2048]{2,1,0:T(8,128)(2,1)}, u32[]{:S(2)}) copy-start(bf16[1,256,2048]{2,1,0:T(8,128)(2,1)} %param.47) | copy-start | bytes 3145732
  7.2 19.9 %copy-start.6 = (f32[2048]{0:T(1024)S(1)}, f32[2048]{0:T(1024)}, u32[]{:S(2)}) copy-start(f32[2048]{0:T(1024)} %param.26) | copy-start | bytes 24580
  7.2 19.6 %copy-start.9 = (f32[256]{0:T(256)S(1)}, f32[256]{0:T(256)}, u32[]{:S(2)}) copy-start(f32[256]{0:T(256)} %param.36) | copy-start | bytes 3076
  7.2 19.8 %copy-start.10 = (f32[256]{0:T(256)S(1)}, f32[256]{0:T(256)}, u32[]{:S(2)}) copy-start(f32[256]{0:T(256)} %param.37) | copy-start | bytes 3076
  7.2 19.9 %copy-start.13 = (bf16[2048,128]{1,0:T(8,128)(2,1)S(1)}, bf16[2048,128]{1,0:T(8,128)(2,1)}, u32[]{:S(2)}) copy-start(bf16[2048,128]{1,0:T(8,128)(2,1)} %param.31) | copy-start | bytes 1572868
  7.2 19.8 %copy-start.15 = (f32[256]{0:T(256)S(1)}, f32[256]{0:T(256)}, u32[]{:S(2)}) copy-start(f32[256]{0:T(256)} %param.33) | copy-start | bytes 3076
  7.2 21.2 %copy-start.3 = (bf16[2048,256]{1,0:T(8,128)(2,1)S(1)}, bf16[2048,256]{1,0:T(8,128)(2,1)}, u32[]{:S(2)}) copy-start(bf16[2048,256]{1,0:T(8,128)(2,1)} %param.30) | copy-start | bytes 3145732
  7.2 78.6 %all-reduce.2.cloned.1.call-start = ((), (), s32[]{:S(2)}) async-start(), calls=%async_computation.3 | async-start | bytes 262144 | tf_op jit(solution)/shard_map/psum | solution.py:145
  28.9 8.7 %copy-start.1 = (f32[32,4,64,64]{3,2,1,0:T(8,128)S(1)}, f32[32,4,64,64]{3,2,1,0:T(8,128)}, u32[]{:S(2)}) copy-start(f32[32,4,64,64]{3,2,1,0:T(8,128)} %param.41) | copy-start | bytes 6291460
  40.3 2.0 %copy-start.2 = (f32[32,4,64,64]{3,2,1,0:T(8,128)}, f32[32,4,64,64]{3,2,1,0:T(8,128)S(1)}, u32[]{:S(2)}) copy-start(f32[32,4,64,64]{3,2,1,0:T(8,128)S(1)} %multiply_add_fusion) | copy-start | bytes 6291460
  40.3 9.5 %copy-start.11 = (f32[256]{0:T(256)S(1)}, f32[256]{0:T(256)}, u32[]{:S(2)}) copy-start(f32[256]{0:T(256)} %param.39) | copy-start | bytes 3076
  40.3 9.6 %copy-start.14 = (f32[4,64]{1,0:T(4,128)S(1)}, f32[4,64]{1,0:T(4,128)}, u32[]{:S(2)}) copy-start(f32[4,64]{1,0:T(4,128)} %param.38) | copy-start | bytes 3076
  40.4 11.1 %copy-start.4 = (bf16[256,2048]{1,0:T(8,128)(2,1)S(1)}, bf16[256,2048]{1,0:T(8,128)(2,1)}, u32[]{:S(2)}) copy-start(bf16[256,2048]{1,0:T(8,128)(2,1)} %param.40) | copy-start | bytes 3145732
  40.4 12.1 %copy-start.7 = (s32[32,4]{0,1:T(4,128)S(1)}, s32[32,4]{0,1:T(4,128)}, u32[]{:S(2)}) copy-start(s32[32,4]{0,1:T(4,128)} %param.43) | copy-start | bytes 1540
  42.3 65.6 %copy-start.5 = (bf16[1,2048,256]{2,1,0:T(8,128)(2,1)S(1)}, bf16[1,2048,256]{2,1,0:T(8,128)(2,1)}, u32[]{:S(2)}) copy-start(bf16[1,2048,256]{2,1,0:T(8,128)(2,1)} %param.45) | copy-start | bytes 3145732
  52.4 79.1 %reduce-scatter.2.cloned.1.call-start = ((), (), s32[]{:S(2)}) async-start(), calls=%async_computation.4 | async-start | bytes 983040 | tf_op jit(solution)/shard_map/reduce_scatter | solution.py:187
  85.8 22.5 %copy-start.12 = (bf16[1,2048,256]{2,1,0:T(8,128)(2,1)S(1)}, bf16[1,2048,256]{2,1,0:T(8,128)(2,1)}, u32[]{:S(2)}) copy-start(bf16[1,2048,256]{2,1,0:T(8,128)(2,1)} %param.46) | copy-start | bytes 3145732
  107.9 29.4 %copy-start.8 = (f32[32,4]{0,1:T(4,128)S(1)}, f32[32,4]{0,1:T(4,128)}, u32[]{:S(2)}) copy-start(f32[32,4]{0,1:T(4,128)} %param.44) | copy-start | bytes 1540
  131.5 13.3 %all-to-all-start.1 = ((bf16[8,24,512]{2,1,0:T(8,128)(2,1)}), bf16[8,24,512]{2,1,0:T(8,128)(2,1)S(1)}, u32[]{:S(2)}, u32[]{:S(2)}) async-start(bf16[8,24,512]{2,1,0:T(8,128)(2,1)} %reduce-scatter.2.cloned.1.call-done), calls=%async_computation.2 | async-start | bytes 393216 | tf_op jit(solution)/shard_map/all_to_all | solution.py:190
Sparse Core Ops, SparseCore 0:
  52.5 33.2 all-reduce.1
  110.1 21.2 reduce-scatter.1
where the time goes:
time: 154 us; the launch traced here: 153 us
  waiting for transfers between devices  60.5 us (39%)
  blocking collectives  33.3 us (22%)
  matrix products  24.5 us (16%)
  between operations  14.4 us (9%)
  other arithmetic  7.99 us (5%)
  local copies, waits for them, and re-layouts  7.04 us (5%)
  starting transfers between devices  5.62 us (4%)
    psum x1, waiting for transfers between devices, shards(): lax.psum(head_terms.astype(jnp.bfloat16), 'tp').astype(jnp.float32)  31.7 us
    reduce_scatter x1, waiting for transfers between devices, shards(): lax.psum_scatter(down_terms.astype(jnp.bfloat16), 'tp', scatter_dimension...  21.4 us
    all_to_all x1, blocking collectives, shards(): lax.all_to_all(outgoing, 'ep', split_axis=0, concat_axis=0, tiled=True)  13.1 us
    dot_general x1, matrix products, head_combiner(): along = jnp.einsum('shij,shj->shi', state, removal, precision=highest)  8.53 us
    all_gather x1, blocking collectives, shards(): lax.all_gather(lax.all_to_all(outgoing, 'ep', split_axis=0, concat_axis=0...  7.59 us
    all_to_all x1, waiting for transfers between devices, shards(): lax.all_to_all(shares, 'ep', split_axis=0, concat_axis=0, tiled=True)  7.37 us
    all_gather x1, blocking collectives, shards(): lax.all_gather(tokens, 'tp', axis=1, tiled=True)  6.85 us
    dot_general x1, matrix products, head_combiner(): jnp.einsum('shij,shj->shi', new_state, receptance_rows, precision=highest)  6.58 us
  transfers between devices with their start and end apart: 3, of which 3 were waited for; matrix products, arithmetic and copies ran while one was open for 1% of the time, Pallas kernels for 0%

commit v1 on v0

v1 whole, which is shorter than its diff:
```python
import math

import jax
import jax.numpy as jnp
from jax import lax
from jax.experimental import pallas as pl
from jax.experimental.pallas import tpu as pltpu
from jax.sharding import PartitionSpec as P

NORM_EPS = 1e-06
GROUP_EPS = 0.00064
KEY_EPS = 1e-06
GATE_LIMIT = 7.0
GATE_SLOPE = 1.702
MESH = pl.DeviceIdType.MESH
F32 = jnp.float32
BF16 = jnp.bfloat16
VMEM = pl.BlockSpec(memory_space=pltpu.VMEM)
ANY = pl.BlockSpec(memory_space=pl.ANY)
HIGHEST = lax.Precision.HIGHEST


def dot(a, b):
    return jnp.dot(a, b, preferred_element_type=F32)


def group_sum(values, width):
    total = values.shape[1]
    row = lax.broadcasted_iota(jnp.int32, (total, total), 0) // width
    col = lax.broadcasted_iota(jnp.int32, (total, total), 1) // width
    ones = jnp.where(row == col, 1.0, 0.0).astype(F32)
    return jnp.dot(values, ones, preferred_element_type=F32, precision=HIGHEST)


def project_kernel(
    tokens, previous, gain, share, offset, removal_scale, damping, self_weight,
    rw, kw, vw, dd, sd, du, su,
    wv_out, dec_out, ra_out, bl_out, v_out, rv_out, sv_out,
    rwv, kwv, vwv, ddv, sdv, duv, suv, gathered,
    weight_sem, local_sem, send_sem, recv_sem,
):
    t = lax.axis_index("tp")
    parts = gathered.shape[1]
    own = tokens.shape[1]
    heads = wv_out.shape[0]
    width = dec_out.shape[2]
    cols = heads * width
    own_cols = pl.ds(pl.multiple_of(t * cols, cols), cols)
    pairs = (
        (rw, rwv), (kw, kwv), (vw, vwv), (dd, ddv), (sd, sdv),
        (du.at[:, own_cols], duv), (su.at[:, own_cols], suv),
    )
    loads = [pltpu.make_async_copy(a, b, weight_sem.at[i]) for i, (a, b) in enumerate(pairs)]
    barrier = pltpu.get_barrier_semaphore()
    for d in range(1, parts):
        pl.semaphore_signal(barrier, inc=1, device_id={"tp": t ^ d}, device_id_type=MESH)
    locals_ = [
        pltpu.make_async_copy(ref, gathered.at[i, t], local_sem.at[i])
        for i, ref in enumerate((tokens, previous))
    ]
    for copy in locals_ + loads:
        copy.start()
    pl.semaphore_wait(barrier, parts - 1)
    copies = []
    for i, ref in enumerate((tokens, previous)):
        for d in range(parts - 1, 0, -1):
            copy = pltpu.make_async_remote_copy(
                src_ref=ref, dst_ref=gathered.at[i, t],
                send_sem=send_sem.at[i, d], recv_sem=recv_sem.at[i, d],
                device_id={"tp": t ^ d}, device_id_type=MESH,
            )
            copy.start()
            copies.append(copy)
    for copy in locals_:
        copy.wait()
    for copy in copies:
        copy.wait()
    squares = 0.0
    for b in range(parts):
        x = gathered[0, b].astype(F32)
        squares = squares + jnp.sum(x * x, axis=-1, keepdims=True)
    scale = lax.rsqrt(squares / (parts * own) + NORM_EPS)
    for copy in loads:
        copy.wait()
    sums = [0.0] * 5
    for b in range(parts):
        span = slice(b * own, (b + 1) * own)
        normed = gathered[0, b].astype(F32) * scale * gain[:, span]
        change = gathered[1, b].astype(F32) - normed
        for m, weight in enumerate((rwv, kwv, vwv, ddv, sdv)):
            shifted = (normed + change * share[m : m + 1, span]).astype(BF16)
            sums[m] = sums[m] + dot(shifted, weight[span, :])
    receptance, key, value = sums[:3]
    decay_pre = offset[...] + dot(jnp.tanh(sums[3]).astype(BF16), duv[...])
    decay = jnp.exp(-math.exp(-0.5) * jax.nn.sigmoid(decay_pre))
    alpha = jax.nn.sigmoid(dot(sums[4].astype(BF16), suv[...]))
    removal = key * removal_scale[...]
    removal = removal * lax.rsqrt(group_sum(removal * removal, width) + KEY_EPS)
    blended = key * (1.0 + (alpha - 1.0) * damping[...])
    strength = removal * alpha
    probe = decay * receptance - group_sum(strength * receptance, width) * removal
    both = receptance * blended
    rv_out[...] = group_sum(both, width) * value
    sv_out[...] = group_sum(both * self_weight[...], width) * value
    for h in range(heads):
        span = slice(h * width, (h + 1) * width)
        wv_out[h] = jnp.concatenate([removal[:, span], probe[:, span]], axis=1)
        dec_out[h] = decay[:, span]
        ra_out[h] = strength[:, span]
        bl_out[h] = blended[:, span]
        v_out[h] = value[:, span]


def project(tokens, previous, gain, share, offset, removal_scale, damping, self_weight, rw, kw, vw, dd, sd, du, su, heads, width, parts):
    rows, own = tokens.shape
    full = parts * own
    cols = heads * width
    head_rows = jax.ShapeDtypeStruct((heads, rows, width), F32)
    flat = jax.ShapeDtypeStruct((rows, cols), F32)
    return pl.pallas_call(
        project_kernel,
        out_shape=[jax.ShapeDtypeStruct((heads, rows, 2 * width), F32)] + [head_rows] * 4 + [flat] * 2,
        in_specs=[VMEM] * 8 + [ANY] * 7,
        out_specs=[VMEM] * 7,
        scratch_shapes=[
            pltpu.VMEM((full, cols), BF16), pltpu.VMEM((full, cols), BF16), pltpu.VMEM((full, cols), BF16),
            pltpu.VMEM(dd.shape, BF16), pltpu.VMEM(sd.shape, BF16),
            pltpu.VMEM((du.shape[0], cols), BF16), pltpu.VMEM((su.shape[0], cols), BF16),
            pltpu.VMEM((2, parts, rows, own), BF16),
            pltpu.SemaphoreType.DMA((7,)),
            pltpu.SemaphoreType.DMA((2,)),
            pltpu.SemaphoreType.DMA((2, parts)),
            pltpu.SemaphoreType.DMA((2, parts)),
        ],
        compiler_params=pltpu.CompilerParams(collective_id=0, has_side_effects=True, vmem_limit_bytes=24 << 20),
        name="gather_project",
    )(tokens, previous, gain, share, offset, removal_scale, damping, self_weight, rw, kw, vw, dd, sd, du, su)


def state_kernel(state, wv, dec, ra, bl, v, rv, sv, gain, new_state, mixed):
    rows, heads, width, _ = state.shape
    wide = 3 * width
    row = lax.broadcasted_iota(jnp.int32, (wide, wide), 0) // width
    col = lax.broadcasted_iota(jnp.int32, (wide, wide), 1) // width
    ones = jnp.where(row == col, 1.0, 0.0).astype(BF16)
    i = lax.broadcasted_iota(jnp.int32, (width, width), 0)
    j = lax.broadcasted_iota(jnp.int32, (width, width), 1)
    eye = jnp.where(i == j, 1.0, 0.0).astype(F32)
    i = lax.broadcasted_iota(jnp.int32, (width, 2 * width), 0)
    j = lax.broadcasted_iota(jnp.int32, (width, 2 * width), 1)
    late = j == i + width
    pieces = []
    for h in range(heads):
        block = state[:, h]
        twice = jnp.concatenate([block, block], axis=2)
        products = (twice * wv[h][:, None, :]).astype(BF16)
        spread = (eye[None] * v[h][:, None, :]).astype(BF16)
        left = jnp.concatenate([products, spread], axis=2)
        total = dot(left.reshape(rows * width, wide), ones).reshape(rows, width, wide)
        along = total[:, :, :width]
        columns = total[:, :, 2 * width :]
        new_state[:, h] = block * dec[h][:, None, :] - along * ra[h][:, None, :] + columns * bl[h][:, None, :]
        picked = jnp.sum(jnp.where(late[None], total[:, :, : 2 * width], 0.0), axis=1)
        readout = picked[:, width:] + rv[:, h * width : (h + 1) * width]
        centered = readout - jnp.mean(readout, axis=-1, keepdims=True)
        variance = jnp.mean(centered * centered, axis=-1, keepdims=True)
        pieces.append(centered * lax.rsqrt(variance + GROUP_EPS))
    mixed[...] = jnp.concatenate(pieces, axis=1) * gain[...] + sv[...]


def update_state(state, wv, dec, ra, bl, v, rv, sv, gain):
    seqs, heads, width, _ = state.shape
    rows = 8
    cols = heads * width
    head_block = pl.BlockSpec((heads, rows, width), lambda s: (0, s, 0))
    flat_block = pl.BlockSpec((rows, cols), lambda s: (s, 0))
    state_block = pl.BlockSpec((rows, heads, width, width), lambda s: (s, 0, 0, 0))
    return pl.pallas_call(
        state_kernel,
        grid=(seqs // rows,),
        out_shape=[jax.ShapeDtypeStruct(state.shape, F32), jax.ShapeDtypeStruct((seqs, cols), F32)],
        in_specs=[
            state_block,
            pl.BlockSpec((heads, rows, 2 * width), lambda s: (0, s, 0)),
            head_block, head_block, head_block, head_block, flat_block, flat_block,
            pl.BlockSpec((1, cols), lambda s: (0, 0)),
        ],
        out_specs=[state_block, flat_block],
        compiler_params=pltpu.CompilerParams(vmem_limit_bytes=24 << 20),
        name="state_update",
    )(state, wv, dec, ra, bl, v, rv, sv, gain)


def repeat(count, body):
    if count <= 8:
        for d in range(count):
            body(d)
    else:
        lax.fori_loop(0, count, lambda d, c: (body(d), c)[1], 0)


def expert_kernel(
    mixed, tokens, gain, dispatch, combine, ow, gw, uw, dw,
    out,
    owv, gwv, uwv, dwv, terms, terms_in, residual, outgoing, arrived,
    down, partner_in, partner_last, cross_out, cross_in, shares, returned,
    weight_sem, terms_send, terms_recv, go_send, go_recv, own_sem,
    x_send, x_recv, p_send, p_recv, f_send, f_recv,
    h_send, h_recv, l_send, l_recv, c_send, c_recv, b_send, b_recv, back_sem,
):
    t = lax.axis_index("tp")
    e = lax.axis_index("ep")
    parts = arrived.shape[0]
    n = returned.shape[0]
    slots = returned.shape[1]
    own = tokens.shape[1]
    partner, cross = t ^ 1, t ^ 2

    def remote(src, dst, send, recv, where):
        return pltpu.make_async_remote_copy(
            src_ref=src, dst_ref=dst, send_sem=send, recv_sem=recv, device_id=where, device_id_type=MESH
        )

    def span(index, size):
        return pl.ds(pl.multiple_of(index * size, size), size)

    barrier = pltpu.get_barrier_semaphore()
    for d in range(1, parts):
        pl.semaphore_signal(barrier, inc=1, device_id={"tp": t ^ d}, device_id_type=MESH)
    repeat(n - 1, lambda d: pl.semaphore_signal(
        barrier, inc=1, device_id={"ep": lax.rem(e + 1 + d, n)}, device_id_type=MESH))
    loads = [
        pltpu.make_async_copy(a, b, weight_sem.at[i])
        for i, (a, b) in enumerate(((ow, owv), (gw.at[0], gwv), (uw.at[0], uwv), (dw.at[0], dwv)))
    ]
    for copy in loads:
        copy.start()

    rows_in = mixed[...].astype(BF16)
    loads[0].wait()
    for d in range(parts - 1, 0, -1):
        terms[d] = dot(rows_in, owv[:, span(t ^ d, own)]).astype(BF16)
    pl.semaphore_wait(barrier, parts - 1 + n - 1)
    sends = [
        remote(terms.at[d], terms_in.at[d], terms_send.at[d], terms_recv.at[d], {"tp": t ^ d})
        for d in range(parts - 1, 0, -1)
    ]
    for copy in sends:
        copy.start()
    total = tokens[...].astype(F32) + dot(rows_in, owv[:, span(t, own)]).astype(BF16).astype(F32)
    for copy in sends:
        copy.wait()
    for d in range(1, parts):
        total = total + terms_in[d].astype(F32)
    residual[...] = total
    outgoing[...] = dot(dispatch[...], total.astype(BF16)).astype(BF16)

    own_copy = pltpu.make_async_copy(outgoing.at[span(e, slots)], arrived.at[t, span(e, slots)], own_sem)
    own_copy.start()

    def go(d):
        where = lax.rem(e + d, n)
        return remote(outgoing.at[span(where, slots)], arrived.at[t, span(e, slots)], go_send.at[d], go_recv.at[d], {"ep": where})

    def source(d):
        return span(lax.rem(e + n - d, n), slots)

    def across(d):
        piece = arrived.at[t, source(d)]
        return remote(piece, piece, x_send.at[d], x_recv.at[d], {"tp": cross})

    def beside(d):
        piece = arrived.at[t, source(d)]
        return remote(piece, piece, p_send.at[d], p_recv.at[d], {"tp": partner})

    def forward(d):
        piece = arrived.at[cross, source(d)]
        return remote(piece, piece, f_send.at[d], f_recv.at[d], {"tp": partner})

    repeat(n - 1, lambda d: go(d + 1).start())
    own_copy.wait()
    across(0).start()
    beside(0).start()

    def pass_on(d):
        go(d + 1).wait_recv()
        across(d + 1).start()
        beside(d + 1).start()
        across(d).wait_recv()
        forward(d).start()

    repeat(n - 1, pass_on)
    across(n - 1).wait_recv()
    forward(n - 1).start()
    for copy in loads[1:]:
        copy.wait()

    def block_sums(block):
        x = arrived[block].astype(F32)
        scaled = (x * gain[:, span(block, own)]).astype(BF16)
        return (
            jnp.sum(x * x, axis=-1, keepdims=True),
            dot(scaled, gwv[span(block, own), :]),
            dot(scaled, uwv[span(block, own), :]),
        )

    def add(a, b):
        return tuple(x + y for x, y in zip(a, b))

    sums = add(block_sums(t), block_sums(cross))
    repeat(n, lambda d: beside(d).wait_recv())
    sums = add(sums, block_sums(partner))
    repeat(n, lambda d: forward(d).wait_recv())
    sums = add(sums, block_sums(t ^ 3))
    squares, gate_pre, up_pre = sums
    scale = lax.rsqrt(squares / (parts * own) + NORM_EPS)
    gate_pre = jnp.minimum(gate_pre * scale, GATE_LIMIT)
    up_pre = jnp.clip(up_pre * scale, -GATE_LIMIT, GATE_LIMIT)
    activation = ((up_pre + 1.0) * gate_pre * jax.nn.sigmoid(GATE_SLOPE * gate_pre)).astype(BF16)

    def target(d):
        return span(lax.rem(e + d, n), slots)

    def hand(d):
        return remote(down.at[3, target(d)], partner_in.at[target(d)], h_send.at[d], h_recv.at[d], {"tp": partner})

    def last(d):
        return remote(down.at[1, target(d)], partner_last.at[target(d)], l_send.at[d], l_recv.at[d], {"tp": partner})

    def crossing(d):
        return remote(cross_out.at[target(d)], cross_in.at[target(d)], c_send.at[d], c_recv.at[d], {"tp": cross})

    def back(d):
        return remote(shares.at[target(d)], returned.at[e], b_send.at[d], b_recv.at[d], {"ep": lax.rem(e + d, n)})

    down[3] = dot(activation, dwv[:, span(t ^ 3, own)]).astype(BF16)
    repeat(n, lambda d: hand(d).start())
    down[2] = dot(activation, dwv[:, span(cross, own)]).astype(BF16)

    def pair(d):
        hand(d).wait_recv()
        at = target(d)
        cross_out[at, :] = (down[2, at, :].astype(F32) + partner_in[at, :].astype(F32)).astype(BF16)
        crossing(d).start()

    order = [d % n for d in range(1, n + 1)]
    if n <= 8:
        for d in order:
            pair(d)
    else:
        repeat(n, lambda d: pair(lax.rem(d + 1, n)))
    down[1] = dot(activation, dwv[:, span(partner, own)]).astype(BF16)
    repeat(n, lambda d: last(d).start())
    down[0] = dot(activation, dwv[:, span(t, own)]).astype(BF16)

    def finish(d):
        last(d).wait_recv()
        crossing(d).wait_recv()
        at = target(d)
        shares[at, :] = (
            down[0, at, :].astype(F32) + partner_last[at, :].astype(F32) + cross_in[at, :].astype(F32)
        ).astype(BF16)

    def finish_remote(d):
        finish(d + 1)
        back(d + 1).start()

    repeat(n - 1, finish_remote)
    finish(0)
    own_back = pltpu.make_async_copy(shares.at[span(e, slots)], returned.at[e], back_sem)
    own_back.start()
    own_back.wait()

    def settle(d):
        go(d + 1).wait_send()
        back(d + 1).wait_send()
        back(d + 1).wait_recv()

    def settle_local(d):
        for copy in (across(d), beside(d), forward(d), hand(d), last(d), crossing(d)):
            copy.wait_send()

    repeat(n, settle_local)
    repeat(n - 1, settle)
    back_rows = returned[...].reshape(n * slots, own)
    weights = combine[...]
    high = weights.astype(BF16)
    low = (weights - high.astype(F32)).astype(BF16)
    out[...] = (residual[...] + (dot(high, back_rows) + dot(low, back_rows))).astype(BF16)


def experts_stage(mixed, tokens, gain, dispatch, combine, ow, gw, uw, dw, n, slots, parts):
    rows, own = tokens.shape
    total = n * slots
    dma = pltpu.SemaphoreType.DMA
    block = pltpu.VMEM((total, own), BF16)
    return pl.pallas_call(
        expert_kernel,
        out_shape=jax.ShapeDtypeStruct((rows, own), BF16),
        in_specs=[VMEM] * 5 + [ANY] * 4,
        out_specs=VMEM,
        scratch_shapes=[
            pltpu.VMEM(ow.shape, BF16), pltpu.VMEM(gw.shape[1:], BF16),
            pltpu.VMEM(uw.shape[1:], BF16), pltpu.VMEM(dw.shape[1:], BF16),
            pltpu.VMEM((parts, rows, own), BF16), pltpu.VMEM((parts, rows, own), BF16),
            pltpu.VMEM((rows, own), F32), block,
            pltpu.VMEM((parts, total, own), BF16), pltpu.VMEM((parts, total, own), BF16),
            block, block, block, block, block,
            pltpu.VMEM((n, slots, own), BF16),
            dma((4,)), dma((parts,)), dma((parts,)), dma((n,)), dma((n,)), dma,
        ] + [dma((n,))] * 14 + [dma],
        compiler_params=pltpu.CompilerParams(collective_id=1, has_side_effects=True, vmem_limit_bytes=44 << 20),
        name="experts",
    )(mixed, tokens, gain, dispatch, combine, ow, gw, uw, dw)


def shards(
    tokens, previous, first_norm_gain, token_shift_share, receptance_weight, key_weight, value_weight,
    decay_down_map, decay_up_map, decay_offset, strength_down_map, strength_up_map, removal_key_scale,
    key_damping, self_term_weight, head_norm_gain, output_weight, state, second_norm_gain, routes,
    chosen_expert_weight, expert_gate_weight, expert_up_weight, expert_down_weight,
):
    parts = lax.axis_size("tp")
    n = lax.axis_size("ep")
    heads, width = state.shape[1], state.shape[2]

    def flat(values):
        return values.reshape(1, -1)

    wv, dec, ra, bl, v, rv, sv = project(
        tokens, previous, flat(first_norm_gain), token_shift_share, flat(decay_offset),
        flat(removal_key_scale), flat(key_damping), flat(self_term_weight),
        receptance_weight, key_weight, value_weight, decay_down_map, strength_down_map,
        decay_up_map, strength_up_map, heads, width, parts,
    )
    new_state, mixed = update_state(state, wv, dec, ra, bl, v, rv, sv, flat(head_norm_gain))

    sequences, choices = routes.shape
    capacity = max(2, 3 * sequences * choices // (2 * n))
    slots = min(sequences, -(-capacity // 16) * 16)
    ids = jnp.arange(n, dtype=jnp.int32)
    chosen = routes[:, :, None] == ids[None, None, :]
    named = jnp.any(chosen, axis=1)
    weight = jnp.sum(jnp.where(chosen, chosen_expert_weight[:, :, None], 0.0), axis=1)
    if slots == sequences:
        rank = jnp.broadcast_to(jnp.arange(sequences, dtype=jnp.int32)[:, None], named.shape)
    else:
        rank = jnp.cumsum(named.astype(jnp.int32), axis=0) - 1
    placed = named[:, :, None] & (rank[:, :, None] == jnp.arange(slots, dtype=jnp.int32)[None, None, :])
    placed = placed.reshape(sequences, n * slots)
    dispatch = placed.T.astype(BF16)
    combine = jnp.where(placed, jnp.repeat(weight, slots, axis=1), 0.0)
    layer_out = experts_stage(
        mixed, tokens, flat(second_norm_gain), dispatch, combine,
        output_weight, expert_gate_weight, expert_up_weight, expert_down_weight, n, slots, parts,
    )
    return (layer_out, new_state)


def solution(mesh):
    in_specs = (
        P("ep", "tp"), P("ep", "tp"), P(), P(), P(None, "tp"), P(None, "tp"), P(None, "tp"), P(), P(),
        P("tp"), P(), P(), P("tp"), P("tp"), P("tp", None), P("tp"), P("tp", None),
        P("ep", "tp", None, None), P(), P("ep", None), P("ep", None),
        P("ep", None, "tp"), P("ep", None, "tp"), P("ep", "tp", None),
    )
    out_specs = (P("ep", "tp"), P("ep", "tp", None, None))
    return jax.shard_map(shards, mesh=mesh, in_specs=in_specs, out_specs=out_specs, check_vma=False)
```

time: 154 us -> 69.5 us (0.45)
  waiting for transfers between devices: 60.5 us -> 0 us
  Pallas kernels: 0 us -> 51.5 us
  blocking collectives: 33.3 us -> 0 us
  matrix products: 24.5 us -> 0 us
  between operations: 14.4 us -> 0.81 us
  local copies, waits for them, and re-layouts: 7.04 us -> 16.5 us
  other arithmetic: 7.99 us -> 0.04 us
  starting transfers between devices: 5.62 us -> 0 us
    pallas_call x0 -> x3, Pallas kernels: none -> 51.5 us  [the longest x1 37.8 us: experts_stage(): pl.pallas_call(expert_kernel, out_shape=jax.ShapeDtypeStruct((rows, own),...]
    psum x1 -> x0, waiting for transfers between devices: 31.7 us -> none  [shards(): lax.psum(head_terms.astype(jnp.bfloat16), 'tp').astype(jnp.float32)]
    dot_general x12 -> x0, matrix products: 24.5 us -> none  [the longest x1 8.53 us: head_combiner(): along = jnp.einsum('shij,shj->shi', state, removal, precision=highest)]
    reduce_scatter x1 -> x0, waiting for transfers between devices: 21.4 us -> none  [shards(): lax.psum_scatter(down_terms.astype(jnp.bfloat16), 'tp', scatter_dimension...]
    all_gather x3 -> x0, blocking collectives: 20.2 us -> none  [the longest x1 7.59 us: shards(): lax.all_gather(lax.all_to_all(outgoing, 'ep', split_axis=0, concat_axis=0...]
    all_to_all x1 -> x0, blocking collectives: 13.1 us -> none  [shards(): lax.all_to_all(outgoing, 'ep', split_axis=0, concat_axis=0, tiled=True)]
    unnamed x34 -> x49, local copies, waits for them, and re-layouts: 2.22 us -> 15 us
    all_to_all x1 -> x0, waiting for transfers between devices: 7.37 us -> none  [shards(): lax.all_to_all(shares, 'ep', split_axis=0, concat_axis=0, tiled=True)]
  transfers between devices with their start and end apart: 3 -> 0, of which waited for: 3 -> 0; matrix products, arithmetic and copies ran while one was open for 1% -> 0% of each run, Pallas kernels for 0% -> 0%
where the time goes in v1:
time: 69.5 us; the launch traced here: 68.9 us
  Pallas kernels  51.5 us (74%)
  local copies, waits for them, and re-layouts  16.5 us (24%)
  between operations  0.81 us (1%)
    pallas_call x1, Pallas kernels, experts_stage(): pl.pallas_call(expert_kernel, out_shape=jax.ShapeDtypeStruct((rows, own),...  37.8 us
    unnamed x49, local copies, waits for them, and re-layouts  15 us
    pallas_call x1, Pallas kernels, project(): pl.pallas_call(project_kernel, out_shape=[jax.ShapeDtypeStruct((heads, ro...  9.06 us
    pallas_call x1, Pallas kernels, update_state(): pl.pallas_call(state_kernel, grid=(seqs // rows,), out_shape=[jax.ShapeDt...  4.62 us

profile of v1, /device:TPU:0, one launch (start us, length us, event | category | flops | bytes accessed | tf_op | source)
XLA Modules:
  0.0 68.9 jit_solution(4548900544303448517)
XLA Ops:
  0.6 0.0 copy-start.18
  0.6 0.8 %reshape.39.self_weight = f32[1,256]{1,0:T(1,128)S(1)} reshape(f32[4,64]{1,0:T(4,128)} %param.38) | data formatting | bytes 2048 | tf_op jit(solution)/shard_map/reshape | solution.py:428
  1.4 0.0 copy-start
  1.4 1.4 %copy-done.1 = bf16[2048,256]{1,0:T(8,128)(2,1)S(1)} copy-done((bf16[2048,256]{1,0:T(8,128)(2,1)S(1)}, bf16[2048,256]{1,0:T(8,128)(2,1)}, u32[]{:S(2)}) %copy-start.1) | copy-done | bytes 1048600
  2.8 0.0 copy-start.2
  2.8 1.4 %copy-done.2 = bf16[2048,256]{1,0:T(8,128)(2,1)S(1)} copy-done((bf16[2048,256]{1,0:T(8,128)(2,1)S(1)}, bf16[2048,256]{1,0:T(8,128)(2,1)}, u32[]{:S(2)}) %copy-start.2) | copy-done | bytes 1048600
  4.2 0.0 copy-start.3
  4.2 1.2 %copy-done.3 = bf16[2048,256]{1,0:T(8,128)(2,1)S(1)} copy-done((bf16[2048,256]{1,0:T(8,128)(2,1)S(1)}, bf16[2048,256]{1,0:T(8,128)(2,1)}, u32[]{:S(2)}) %copy-start.3) | copy-done | bytes 1048600
  5.4 0.0 copy-start.8
  5.4 1.0 %copy-done.8 = bf16[2048,128]{1,0:T(8,128)(2,1)S(1)} copy-done((bf16[2048,128]{1,0:T(8,128)(2,1)S(1)}, bf16[2048,128]{1,0:T(8,128)(2,1)}, u32[]{:S(2)}) %copy-start.8) | copy-done | bytes 524312
  6.5 0.0 copy-start.9
  6.5 1.0 %copy-done.9 = bf16[2048,128]{1,0:T(8,128)(2,1)S(1)} copy-done((bf16[2048,128]{1,0:T(8,128)(2,1)S(1)}, bf16[2048,128]{1,0:T(8,128)(2,1)}, u32[]{:S(2)}) %copy-start.9) | copy-done | bytes 524312
  7.5 0.0 copy-start.10
  7.5 0.9 %copy-done.10 = bf16[128,1024]{1,0:T(8,128)(2,1)S(1)} copy-done((bf16[128,1024]{1,0:T(8,128)(2,1)S(1)}, bf16[128,1024]{1,0:T(8,128)(2,1)}, u32[]{:S(2)}) %copy-start.10) | copy-done | bytes 262168
  8.5 0.9 %copy-done.11 = bf16[128,1024]{1,0:T(8,128)(2,1)S(1)} copy-done((bf16[128,1024]{1,0:T(8,128)(2,1)S(1)}, bf16[128,1024]{1,0:T(8,128)(2,1)}, u32[]{:S(2)}) %copy-start.11) | copy-done | bytes 262168
  9.4 0.8 %copy-done.12 = bf16[32,512]{1,0:T(8,128)(2,1)S(1)} copy-done((bf16[32,512]{1,0:T(8,128)(2,1)S(1)}, bf16[32,512]{1,0:T(8,128)(2,1)}, u32[]{:S(2)}) %copy-start.12) | copy-done | bytes 32792
  10.2 0.8 %copy-done.14 = f32[5,2048]{1,0:T(8,128)S(1)} copy-done((f32[5,2048]{1,0:T(8,128)S(1)}, f32[5,2048]{1,0:T(8,128)}, u32[]{:S(2)}) %copy-start.14) | copy-done | bytes 40984
  11.0 0.8 %copy-done.15 = bf16[32,512]{1,0:T(8,128)(2,1)S(1)} copy-done((bf16[32,512]{1,0:T(8,128)(2,1)S(1)}, bf16[32,512]{1,0:T(8,128)(2,1)}, u32[]{:S(2)}) %copy-start.15) | copy-done | bytes 32792
  11.8 0.7 %copy-done.16 = f32[2048]{0:T(1024)S(1)} copy-done((f32[2048]{0:T(1024)S(1)}, f32[2048]{0:T(1024)}, u32[]{:S(2)}) %copy-start.16) | copy-done | bytes 8216
  12.5 0.7 copy-done.19
  13.2 0.7 copy-done.20
  13.8 0.7 copy-done.21
  14.5 0.0 copy-start.6
  14.5 0.0 copy-start.13
  14.5 0.0 copy-start.17
  14.6 9.1 %gather_project.1 = (f32[4,32,128]{2,1,0:T(8,128)S(1)}, f32[4,32,64]{2,1,0:T(8,128)S(1)}, f32[4,32,64]{2,1,0:T(8,128)S(1)}, f32[4,32,64]{2,1,0:T(8,128)S(1)}, f3...) custom-call(bf16[32,512]{1,0:T(8,128)(2,1)S(1)} %copy-done.12, ...), custom_call_target="tpu_custom_call" | custom-call | tf_op jit(solution)/shard_map/gather_project/pallas_call | solution.py:120
  23.6 0.0 copy-done.18
  23.6 0.0 copy-done
  23.6 4.6 %state_update.1 = (f32[32,4,64,64]{3,2,1,0:T(8,128)}, f32[32,256]{1,0:T(8,128)S(1)}) custom-call(f32[32,4,64,64]{3,2,1,0:T(8,128)S(1)} %copy-done, f32[4,32,128]{2,1,0:T(8,128)S(1)} %get-tuple-element.11.wv, f32[4,32,64]{2,1,0:T(8,128)S(1)} %get-tuple-element.12.dec, f32[4,32,64]{2,1,0:T(8,128)S(1)} %get-tuple-element.13.ra, ...), custom_call_target="tpu_custom_call" | custom-call | tf_op jit(solution)/shard_map/state_update/pallas_call | solution.py:178
  28.3 0.0 copy-done.22
  28.3 0.1 copy.29
  28.4 0.1 and.11
  28.5 0.1 and.12
  28.6 0.1 eq.30
  28.7 0.0 copy-done.23
  28.7 0.1 copy.30
  28.8 0.1 broadcast_in_dim.27
  28.9 0.1 reshape.42
  29.0 0.1 copy.31.dispatch
  29.1 0.0 copy-done.4
  29.1 0.0 copy-done.5
  29.2 0.0 copy-done.6
  29.2 0.0 copy-done.13
  29.2 0.0 copy-done.17
  29.2 0.0 copy-start.7
  29.2 1.2 %copy-done.7 = bf16[1,256,2048]{2,1,0:T(8,128)(2,1)S(1)} copy-done((bf16[1,256,2048]{2,1,0:T(8,128)(2,1)S(1)}, bf16[1,256,2048]{2,1,0:T(8,128)(2,1)}, u32[]{:S(2)}) %copy-start.7) | copy-done | bytes 1048600
  30.4 37.8 %experts.1 = bf16[32,512]{1,0:T(8,128)(2,1)S(1)} custom-call(f32[32,256]{1,0:T(8,128)S(1)} %get-tuple-element.18.mixed, bf16[32,512]{1,0:T(8,128)(2,1)S(1)} %copy-done.13, f32[1,2048]{1,0:T(1,128)S(1)} %bitcast.9, bf16[256,32]{1,0:T(8,128)(2,1)S(1)} %copy.31.dispatch, f32[32,256]{1,0:T(8,128)S(1)} %fusion.1.combine, bf16[256,2048]{1,0:T(8,128)(2,1)S(1)} %copy-done.4, ...), custom_call_target="tpu_custom_call" | custom-call | tf_op jit(solution)/shard_map/experts/pallas_call | solution.py:397
  68.3 0.6 copy.33
  (18 shorter events, 0.1 us)
Async XLA Ops:
  0.6 23.0 %copy-start.18 = (f32[256]{0:T(256)S(1)}, f32[256]{0:T(256)}, u32[]{:S(2)}) copy-start(f32[256]{0:T(256)} %param.39) | copy-start | bytes 3076
  1.4 22.2 %copy-start = (f32[32,4,64,64]{3,2,1,0:T(8,128)S(1)}, f32[32,4,64,64]{3,2,1,0:T(8,128)}, u32[]{:S(2)}) copy-start(f32[32,4,64,64]{3,2,1,0:T(8,128)} %state.1) | copy-start | bytes 6291460
  1.4 1.4 %copy-start.1 = (bf16[2048,256]{1,0:T(8,128)(2,1)S(1)}, bf16[2048,256]{1,0:T(8,128)(2,1)}, u32[]{:S(2)}) copy-start(bf16[2048,256]{1,0:T(8,128)(2,1)} %rw.1) | copy-start | bytes 3145732
  2.8 1.4 %copy-start.2 = (bf16[2048,256]{1,0:T(8,128)(2,1)S(1)}, bf16[2048,256]{1,0:T(8,128)(2,1)}, u32[]{:S(2)}) copy-start(bf16[2048,256]{1,0:T(8,128)(2,1)} %kw.1) | copy-start | bytes 3145732
  4.2 1.2 %copy-start.3 = (bf16[2048,256]{1,0:T(8,128)(2,1)S(1)}, bf16[2048,256]{1,0:T(8,128)(2,1)}, u32[]{:S(2)}) copy-start(bf16[2048,256]{1,0:T(8,128)(2,1)} %vw.1) | copy-start | bytes 3145732
  5.4 1.0 %copy-start.8 = (bf16[2048,128]{1,0:T(8,128)(2,1)S(1)}, bf16[2048,128]{1,0:T(8,128)(2,1)}, u32[]{:S(2)}) copy-start(bf16[2048,128]{1,0:T(8,128)(2,1)} %dd.1) | copy-start | bytes 1572868
  6.5 1.0 %copy-start.9 = (bf16[2048,128]{1,0:T(8,128)(2,1)S(1)}, bf16[2048,128]{1,0:T(8,128)(2,1)}, u32[]{:S(2)}) copy-start(bf16[2048,128]{1,0:T(8,128)(2,1)} %sd.1) | copy-start | bytes 1572868
  7.5 0.9 %copy-start.10 = (bf16[128,1024]{1,0:T(8,128)(2,1)S(1)}, bf16[128,1024]{1,0:T(8,128)(2,1)}, u32[]{:S(2)}) copy-start(bf16[128,1024]{1,0:T(8,128)(2,1)} %du.1) | copy-start | bytes 786436
  8.5 0.9 %copy-start.11 = (bf16[128,1024]{1,0:T(8,128)(2,1)S(1)}, bf16[128,1024]{1,0:T(8,128)(2,1)}, u32[]{:S(2)}) copy-start(bf16[128,1024]{1,0:T(8,128)(2,1)} %su.1) | copy-start | bytes 786436
  9.4 0.8 %copy-start.12 = (bf16[32,512]{1,0:T(8,128)(2,1)S(1)}, bf16[32,512]{1,0:T(8,128)(2,1)}, u32[]{:S(2)}) copy-start(bf16[32,512]{1,0:T(8,128)(2,1)} %tokens.3) | copy-start | bytes 98308
  10.2 0.8 %copy-start.14 = (f32[5,2048]{1,0:T(8,128)S(1)}, f32[5,2048]{1,0:T(8,128)}, u32[]{:S(2)}) copy-start(f32[5,2048]{1,0:T(8,128)} %share.1) | copy-start | bytes 122884
  11.0 0.8 %copy-start.15 = (bf16[32,512]{1,0:T(8,128)(2,1)S(1)}, bf16[32,512]{1,0:T(8,128)(2,1)}, u32[]{:S(2)}) copy-start(bf16[32,512]{1,0:T(8,128)(2,1)} %previous.1) | copy-start | bytes 98308
  11.8 0.7 %copy-start.16 = (f32[2048]{0:T(1024)S(1)}, f32[2048]{0:T(1024)}, u32[]{:S(2)}) copy-start(f32[2048]{0:T(1024)} %param.26) | copy-start | bytes 24580
  12.5 0.7 copy-start.19
  13.2 0.7 copy-start.20
  13.8 0.7 copy-start.21
  14.5 13.8 %copy-start.22 = (s32[32,4]{0,1:T(4,128)S(1)}, s32[32,4]{0,1:T(4,128)}, u32[]{:S(2)}) copy-start(s32[32,4]{0,1:T(4,128)} %param.43) | copy-start | bytes 1540
  14.5 14.2 %copy-start.23 = (f32[32,4]{0,1:T(4,128)S(1)}, f32[32,4]{0,1:T(4,128)}, u32[]{:S(2)}) copy-start(f32[32,4]{0,1:T(4,128)} %param.44) | copy-start | bytes 1540
  14.5 14.6 %copy-start.4 = (bf16[256,2048]{1,0:T(8,128)(2,1)S(1)}, bf16[256,2048]{1,0:T(8,128)(2,1)}, u32[]{:S(2)}) copy-start(bf16[256,2048]{1,0:T(8,128)(2,1)} %ow.1) | copy-start | bytes 3145732
  14.5 14.6 %copy-start.5 = (bf16[1,2048,256]{2,1,0:T(8,128)(2,1)S(1)}, bf16[1,2048,256]{2,1,0:T(8,128)(2,1)}, u32[]{:S(2)}) copy-start(bf16[1,2048,256]{2,1,0:T(8,128)(2,1)} %gw.1) | copy-start | bytes 3145732
  14.5 14.6 %copy-start.6 = (bf16[1,2048,256]{2,1,0:T(8,128)(2,1)S(1)}, bf16[1,2048,256]{2,1,0:T(8,128)(2,1)}, u32[]{:S(2)}) copy-start(bf16[1,2048,256]{2,1,0:T(8,128)(2,1)} %uw.1) | copy-start | bytes 3145732
  14.5 14.6 %copy-start.13 = (bf16[32,512]{1,0:T(8,128)(2,1)S(1)}, bf16[32,512]{1,0:T(8,128)(2,1)}, u32[]{:S(2)}) copy-start(bf16[32,512]{1,0:T(8,128)(2,1)} %tokens.3) | copy-start | bytes 98308
  14.5 14.6 %copy-start.17 = (f32[2048]{0:T(1024)S(1)}, f32[2048]{0:T(1024)}, u32[]{:S(2)}) copy-start(f32[2048]{0:T(1024)} %param.42) | copy-start | bytes 24580
  29.2 1.2 %copy-start.7 = (bf16[1,256,2048]{2,1,0:T(8,128)(2,1)S(1)}, bf16[1,256,2048]{2,1,0:T(8,128)(2,1)}, u32[]{:S(2)}) copy-start(bf16[1,256,2048]{2,1,0:T(8,128)(2,1)} %dw.1) | copy-start | bytes 3145732

commit v2 on v1

v2 whole, which is shorter than its diff:
```python
import math

import jax
import jax.numpy as jnp
from jax import lax
from jax.experimental import pallas as pl
from jax.experimental.pallas import tpu as pltpu
from jax.sharding import PartitionSpec as P

NORM_EPS = 1e-06
GROUP_EPS = 0.00064
KEY_EPS = 1e-06
GATE_LIMIT = 7.0
GATE_SLOPE = 1.702
MESH = pl.DeviceIdType.MESH
F32 = jnp.float32
BF16 = jnp.bfloat16
VMEM = pl.BlockSpec(memory_space=pltpu.VMEM)
HBM = pl.BlockSpec(memory_space=pltpu.MemorySpace.HBM)
HIGHEST = lax.Precision.HIGHEST


def dot(a, b):
    return jnp.dot(a, b, preferred_element_type=F32)


def group_sum(values, width):
    total = values.shape[1]
    row = lax.broadcasted_iota(jnp.int32, (total, total), 0) // width
    col = lax.broadcasted_iota(jnp.int32, (total, total), 1) // width
    ones = jnp.where(row == col, 1.0, 0.0).astype(F32)
    return jnp.dot(values, ones, preferred_element_type=F32, precision=HIGHEST)


def project_kernel(
    tokens, previous, gain_in, share_in, offset_in, removal_in, damping_in, self_in,
    rw, kw, vw, dd, sd, du, su,
    wv_out, dec_out, ra_out, bl_out, v_out, rv_out, sv_out,
    gain, share, offset, removal_scale, damping, self_rows,
    rwv, kwv, vwv, ddv, sdv, duv, suv, gathered,
    weight_sem, local_sem, send_sem, recv_sem,
):
    t = lax.axis_index("tp")
    parts = gathered.shape[1]
    own = tokens.shape[1]
    heads = wv_out.shape[0]
    width = dec_out.shape[2]
    cols = heads * width
    own_cols = pl.ds(pl.multiple_of(t * cols, cols), cols)
    pairs = (
        (gain_in, gain), (share_in, share),
        (rw, rwv), (kw, kwv), (vw, vwv), (dd, ddv), (sd, sdv),
        (du.at[:, own_cols], duv), (su.at[:, own_cols], suv),
        (offset_in, offset), (removal_in, removal_scale), (damping_in, damping), (self_in, self_rows),
    )
    loads = [pltpu.make_async_copy(a, b, weight_sem.at[i]) for i, (a, b) in enumerate(pairs)]
    barrier = pltpu.get_barrier_semaphore()
    for d in range(1, parts):
        pl.semaphore_signal(barrier, inc=1, device_id={"tp": t ^ d}, device_id_type=MESH)
    locals_ = [
        pltpu.make_async_copy(ref, gathered.at[i, t], local_sem.at[i])
        for i, ref in enumerate((tokens, previous))
    ]
    for copy in locals_ + loads:
        copy.start()
    pl.semaphore_wait(barrier, parts - 1)
    copies = []
    for i in range(2):
        locals_[i].wait()
        for d in range(parts - 1, 0, -1):
            copy = pltpu.make_async_remote_copy(
                src_ref=gathered.at[i, t], dst_ref=gathered.at[i, t],
                send_sem=send_sem.at[i, d], recv_sem=recv_sem.at[i, d],
                device_id={"tp": t ^ d}, device_id_type=MESH,
            )
            copy.start()
            copies.append(copy)
    for copy in copies:
        copy.wait()
    squares = 0.0
    for b in range(parts):
        x = gathered[0, b].astype(F32)
        squares = squares + jnp.sum(x * x, axis=-1, keepdims=True)
    scale = lax.rsqrt(squares / (parts * own) + NORM_EPS)
    for copy in loads:
        copy.wait()
    sums = [0.0] * 5
    for b in range(parts):
        span = slice(b * own, (b + 1) * own)
        normed = gathered[0, b].astype(F32) * scale * gain[:, span]
        change = gathered[1, b].astype(F32) - normed
        for m, weight in enumerate((rwv, kwv, vwv, ddv, sdv)):
            shifted = (normed + change * share[m : m + 1, span]).astype(BF16)
            sums[m] = sums[m] + dot(shifted, weight[span, :])
    receptance, key, value = sums[:3]
    decay_pre = offset[...] + dot(jnp.tanh(sums[3]).astype(BF16), duv[...])
    decay = jnp.exp(-math.exp(-0.5) * jax.nn.sigmoid(decay_pre))
    alpha = jax.nn.sigmoid(dot(sums[4].astype(BF16), suv[...]))
    removal = key * removal_scale[...]
    removal = removal * lax.rsqrt(group_sum(removal * removal, width) + KEY_EPS)
    blended = key * (1.0 + (alpha - 1.0) * damping[...])
    strength = removal * alpha
    probe = decay * receptance - group_sum(strength * receptance, width) * removal
    both = receptance * blended
    self_weight = jnp.concatenate([self_rows[h : h + 1, :] for h in range(heads)], axis=1)
    rv_out[...] = group_sum(both, width) * value
    sv_out[...] = group_sum(both * self_weight, width) * value
    for h in range(heads):
        span = slice(h * width, (h + 1) * width)
        wv_out[h] = jnp.concatenate([removal[:, span], probe[:, span]], axis=1)
        dec_out[h] = decay[:, span]
        ra_out[h] = strength[:, span]
        bl_out[h] = blended[:, span]
        v_out[h] = value[:, span]


def project(tokens, previous, gain, share, offset, removal_scale, damping, self_weight, rw, kw, vw, dd, sd, du, su, heads, width, parts):
    rows, own = tokens.shape
    full = parts * own
    cols = heads * width
    head_rows = jax.ShapeDtypeStruct((heads, rows, width), F32)
    flat = jax.ShapeDtypeStruct((rows, cols), F32)
    return pl.pallas_call(
        project_kernel,
        out_shape=[jax.ShapeDtypeStruct((heads, rows, 2 * width), F32)] + [head_rows] * 4 + [flat] * 2,
        in_specs=[HBM] * 15,
        out_specs=[VMEM] * 7,
        scratch_shapes=[
            pltpu.VMEM(gain.shape, F32), pltpu.VMEM(share.shape, F32), pltpu.VMEM(offset.shape, F32),
            pltpu.VMEM(removal_scale.shape, F32), pltpu.VMEM(damping.shape, F32), pltpu.VMEM(self_weight.shape, F32),
            pltpu.VMEM((full, cols), BF16), pltpu.VMEM((full, cols), BF16), pltpu.VMEM((full, cols), BF16),
            pltpu.VMEM(dd.shape, BF16), pltpu.VMEM(sd.shape, BF16),
            pltpu.VMEM((du.shape[0], cols), BF16), pltpu.VMEM((su.shape[0], cols), BF16),
            pltpu.VMEM((2, parts, rows, own), BF16),
            pltpu.SemaphoreType.DMA((13,)),
            pltpu.SemaphoreType.DMA((2,)),
            pltpu.SemaphoreType.DMA((2, parts)),
            pltpu.SemaphoreType.DMA((2, parts)),
        ],
        compiler_params=pltpu.CompilerParams(collective_id=0, has_side_effects=True, vmem_limit_bytes=67_000_000),
        name="gather_project",
    )(tokens, previous, gain, share, offset, removal_scale, damping, self_weight, rw, kw, vw, dd, sd, du, su)


def state_kernel(state, wv, dec, ra, bl, v, rv, sv, gain, new_state, mixed):
    rows, heads, width, _ = state.shape
    wide = 3 * width
    row = lax.broadcasted_iota(jnp.int32, (wide, wide), 0) // width
    col = lax.broadcasted_iota(jnp.int32, (wide, wide), 1) // width
    ones = jnp.where(row == col, 1.0, 0.0).astype(BF16)
    i = lax.broadcasted_iota(jnp.int32, (width, width), 0)
    j = lax.broadcasted_iota(jnp.int32, (width, width), 1)
    eye = jnp.where(i == j, 1.0, 0.0).astype(F32)
    i = lax.broadcasted_iota(jnp.int32, (width, 2 * width), 0)
    j = lax.broadcasted_iota(jnp.int32, (width, 2 * width), 1)
    late = j == i + width
    pieces = []
    for h in range(heads):
        block = state[:, h]
        twice = jnp.concatenate([block, block], axis=2)
        products = (twice * wv[h][:, None, :]).astype(BF16)
        spread = (eye[None] * v[h][:, None, :]).astype(BF16)
        left = jnp.concatenate([products, spread], axis=2)
        total = dot(left.reshape(rows * width, wide), ones).reshape(rows, width, wide)
        along = total[:, :, :width]
        columns = total[:, :, 2 * width :]
        new_state[:, h] = block * dec[h][:, None, :] - along * ra[h][:, None, :] + columns * bl[h][:, None, :]
        picked = jnp.sum(jnp.where(late[None], total[:, :, : 2 * width], 0.0), axis=1)
        readout = picked[:, width:] + rv[:, h * width : (h + 1) * width]
        centered = readout - jnp.mean(readout, axis=-1, keepdims=True)
        variance = jnp.mean(centered * centered, axis=-1, keepdims=True)
        pieces.append(centered * lax.rsqrt(variance + GROUP_EPS))
    mixed[...] = jnp.concatenate(pieces, axis=1) * gain[...] + sv[...]


def update_state(state, wv, dec, ra, bl, v, rv, sv, gain):
    seqs, heads, width, _ = state.shape
    rows = 8
    cols = heads * width
    head_block = pl.BlockSpec((heads, rows, width), lambda s: (0, s, 0))
    flat_block = pl.BlockSpec((rows, cols), lambda s: (s, 0))
    state_block = pl.BlockSpec((rows, heads, width, width), lambda s: (s, 0, 0, 0))
    return pl.pallas_call(
        state_kernel,
        grid=(seqs // rows,),
        out_shape=[jax.ShapeDtypeStruct(state.shape, F32), jax.ShapeDtypeStruct((seqs, cols), F32)],
        in_specs=[
            state_block,
            pl.BlockSpec((heads, rows, 2 * width), lambda s: (0, s, 0)),
            head_block, head_block, head_block, head_block, flat_block, flat_block,
            pl.BlockSpec((1, cols), lambda s: (0, 0)),
        ],
        out_specs=[state_block, flat_block],
        compiler_params=pltpu.CompilerParams(vmem_limit_bytes=67_000_000),
        name="state_update",
    )(state, wv, dec, ra, bl, v, rv, sv, gain)


def repeat(first, end, body):
    if end - first <= 8:
        for d in range(first, end):
            body(d)
    else:
        lax.fori_loop(first, end, lambda d, c: (body(d), c)[1], 0)


def expert_kernel(
    mixed_in, tokens_in, gain_in, routes_in, chosen_in, ow_in, gw, uw, dw,
    out,
    mixed, tokens, gain, routes, chosen, ow, gwv, uwv, dwv, terms, terms_in, residual, outgoing, arrived,
    down, partner_in, partner_last, cross_out, cross_in, shares, returned, combine,
    weight_sem, terms_send, terms_recv, own_sem,
    go_send, go_recv, x_send, x_recv, p_send, p_recv, f_send, f_recv,
    h_send, h_recv, l_send, l_recv, c_send, c_recv, b_send, b_recv,
):
    t = lax.axis_index("tp")
    e = lax.axis_index("ep")
    parts = arrived.shape[0]
    n = go_send.shape[0]
    total_slots, own = returned.shape
    slots = total_slots // n
    seqs = tokens.shape[0]
    dense = slots == seqs
    partner, cross = t ^ 1, t ^ 2

    def remote(src, dst, send, recv, where):
        return pltpu.make_async_remote_copy(
            src_ref=src, dst_ref=dst, send_sem=send, recv_sem=recv, device_id=where, device_id_type=MESH
        )

    def span(index, size):
        if isinstance(index, int):
            return pl.ds(index * size, size)
        return pl.ds(pl.multiple_of(index * size, size), size)

    barrier = pltpu.get_barrier_semaphore()
    for d in range(1, parts):
        pl.semaphore_signal(barrier, inc=1, device_id={"tp": t ^ d}, device_id_type=MESH)
    repeat(1, n, lambda d: pl.semaphore_signal(
        barrier, inc=1, device_id={"ep": lax.rem(e + d, n)}, device_id_type=MESH))
    loads = [
        pltpu.make_async_copy(a, b, weight_sem.at[i])
        for i, (a, b) in enumerate((
            (mixed_in, mixed), (ow_in, ow), (tokens_in, tokens), (routes_in, routes), (chosen_in, chosen),
            (gain_in, gain), (gw.at[0], gwv), (uw.at[0], uwv), (dw.at[0], dwv),
        ))
    ]
    for copy in loads:
        copy.start()

    for copy in loads[:5]:
        copy.wait()
    rows_in = mixed[...].astype(BF16)
    for d in range(parts - 1, 0, -1):
        terms[d] = dot(rows_in, ow[:, span(t ^ d, own)]).astype(BF16)
    pl.semaphore_wait(barrier, parts - 1 + n - 1)
    sends = [
        remote(terms.at[d], terms_in.at[d], terms_send.at[d], terms_recv.at[d], {"tp": t ^ d})
        for d in range(parts - 1, 0, -1)
    ]
    for copy in sends:
        copy.start()
    total = tokens[...].astype(F32) + dot(rows_in, ow[:, span(t, own)]).astype(BF16).astype(F32)

    column = lax.broadcasted_iota(jnp.int32, (total_slots, seqs), 0)
    sequence = lax.broadcasted_iota(jnp.int32, (total_slots, seqs), 1)
    expert = lax.rem(e + column // slots, n)
    weight = jnp.zeros((total_slots, seqs), F32)
    named = jnp.zeros((total_slots, seqs), F32)
    for k in range(routes.shape[0]):
        hit = routes[k : k + 1, :] == expert
        weight = weight + jnp.where(hit, chosen[k : k + 1, :], 0.0)
        named = named + jnp.where(hit, 1.0, 0.0)
    if dense:
        placed = jnp.where(sequence == column % slots, named, 0.0)
    else:
        i = lax.broadcasted_iota(jnp.int32, (seqs, seqs), 0)
        j = lax.broadcasted_iota(jnp.int32, (seqs, seqs), 1)
        before = jnp.where(i < j, 1.0, 0.0).astype(BF16)
        rank = dot(named.astype(BF16), before)
        placed = jnp.where(rank == (column % slots).astype(F32), named, 0.0)
    combine[...] = (placed * weight).T

    for copy in sends:
        copy.wait()
    for d in range(1, parts):
        total = total + terms_in[d].astype(F32)
    residual[...] = total
    if dense:
        outgoing[...] = total.astype(BF16)
    else:
        outgoing[...] = dot(placed.astype(BF16), total.astype(BF16)).astype(BF16)

    def outgoing_block(d):
        return outgoing if dense else outgoing.at[span(d, slots)]

    def go(d):
        return remote(
            outgoing_block(d), arrived.at[t, span(d, slots)], go_send.at[d], go_recv.at[d],
            {"ep": lax.rem(e + d, n)},
        )

    def across(d):
        piece = arrived.at[t, span(d, slots)]
        return remote(piece, piece, x_send.at[d], x_recv.at[d], {"tp": cross})

    def beside(d):
        piece = arrived.at[t, span(d, slots)]
        return remote(piece, piece, p_send.at[d], p_recv.at[d], {"tp": partner})

    def forward(d):
        piece = arrived.at[cross, span(d, slots)]
        return remote(piece, piece, f_send.at[d], f_recv.at[d], {"tp": partner})

    def hand(d):
        at = span(d, slots)
        return remote(down.at[3, at], partner_in.at[at], h_send.at[d], h_recv.at[d], {"tp": partner})

    def last(d):
        at = span(d, slots)
        return remote(down.at[1, at], partner_last.at[at], l_send.at[d], l_recv.at[d], {"tp": partner})

    def crossing(d):
        at = span(d, slots)
        return remote(cross_out.at[at], cross_in.at[at], c_send.at[d], c_recv.at[d], {"tp": cross})

    def back(d):
        at = span(d, slots)
        return remote(shares.at[at], returned.at[at], b_send.at[d], b_recv.at[d], {"ep": lax.rem(e + n - d, n)})

    def spread(d):
        across(d).start()
        beside(d).start()

    def pass_on(d):
        across(d).wait_recv()
        forward(d).start()

    def arrive(first, end):
        def one(d):
            go(d).wait_recv()
            spread(d)
            pass_on(d - 1)

        repeat(max(first, 1), end, one)

    def block_sums(block, rows):
        x = arrived[block, rows, :].astype(F32)
        scaled = (x * gain[:, span(block, own)]).astype(BF16)
        return (
            jnp.sum(x * x, axis=-1, keepdims=True),
            dot(scaled, gwv[span(block, own), :]),
            dot(scaled, uwv[span(block, own), :]),
        )

    def add(a, b):
        return tuple(x + y for x, y in zip(a, b))

    def expert_rows(first, end):
        rows = pl.ds(first * slots, (end - first) * slots)
        sums = add(block_sums(t, rows), block_sums(cross, rows))
        repeat(first, end, lambda d: beside(d).wait_recv())
        sums = add(sums, block_sums(partner, rows))
        repeat(first, end, lambda d: forward(d).wait_recv())
        squares, gate_pre, up_pre = add(sums, block_sums(t ^ 3, rows))
        scale = lax.rsqrt(squares / (parts * own) + NORM_EPS)
        gate_pre = jnp.minimum(gate_pre * scale, GATE_LIMIT)
        up_pre = jnp.clip(up_pre * scale, -GATE_LIMIT, GATE_LIMIT)
        activation = ((up_pre + 1.0) * gate_pre * jax.nn.sigmoid(GATE_SLOPE * gate_pre)).astype(BF16)
        down[3, rows, :] = dot(activation, dwv[:, span(t ^ 3, own)]).astype(BF16)
        repeat(first, end, lambda d: hand(d).start())
        down[2, rows, :] = dot(activation, dwv[:, span(cross, own)]).astype(BF16)
        down[1, rows, :] = dot(activation, dwv[:, span(partner, own)]).astype(BF16)
        repeat(first, end, lambda d: last(d).start())
        down[0, rows, :] = dot(activation, dwv[:, span(t, own)]).astype(BF16)

    def pair(d):
        hand(d).wait_recv()
        at = span(d, slots)
        cross_out[at, :] = (down[2, at, :].astype(F32) + partner_in[at, :].astype(F32)).astype(BF16)
        crossing(d).start()

    def finish(d):
        last(d).wait_recv()
        crossing(d).wait_recv()
        at = span(d, slots)
        return (
            down[0, at, :].astype(F32) + partner_last[at, :].astype(F32) + cross_in[at, :].astype(F32)
        ).astype(BF16)

    def send_back(d):
        shares[span(d, slots), :] = finish(d)
        back(d).start()

    own_copy = pltpu.make_async_copy(outgoing_block(0), arrived.at[t, span(0, slots)], own_sem)
    own_copy.start()
    repeat(1, n, lambda d: go(d).start())
    own_copy.wait()
    spread(0)
    half = n // 2
    arrive(0, half)
    pass_on(half - 1)
    for copy in loads[5:]:
        copy.wait()
    expert_rows(0, half)

    def arrive_first(d):
        go(d).wait_recv()
        spread(d)

    arrive_first(half)
    repeat(0, half, pair)
    arrive(half + 1, n)
    pass_on(n - 1)
    repeat(1, half, send_back)
    expert_rows(half, n)
    repeat(half, n, pair)
    returned[pl.ds(0, slots), :] = finish(0)
    repeat(half, n, send_back)

    def settle(d):
        go(d).wait_send()
        back(d).wait_send()

    def settle_local(d):
        for copy in (across(d), beside(d), forward(d), hand(d), last(d), crossing(d)):
            copy.wait_send()

    repeat(0, n, settle_local)
    repeat(1, n, settle)
    weights = combine[...]
    high = weights.astype(BF16)
    low = (weights - high.astype(F32)).astype(BF16)
    repeat(1, n, lambda d: back(d).wait_recv())
    rows_back = returned[...]
    out[...] = (residual[...] + (dot(high, rows_back) + dot(low, rows_back))).astype(BF16)


def experts_stage(mixed, tokens, gain, routes, chosen, ow, gw, uw, dw, n, slots, parts):
    rows, own = tokens.shape
    total = n * slots
    dma = pltpu.SemaphoreType.DMA
    block = pltpu.VMEM((total, own), BF16)
    return pl.pallas_call(
        expert_kernel,
        out_shape=jax.ShapeDtypeStruct((rows, own), BF16),
        in_specs=[HBM] * 9,
        out_specs=VMEM,
        scratch_shapes=[
            pltpu.VMEM(mixed.shape, F32), pltpu.VMEM(tokens.shape, BF16), pltpu.VMEM(gain.shape, F32),
            pltpu.VMEM(routes.shape, jnp.int32), pltpu.VMEM(chosen.shape, F32), pltpu.VMEM(ow.shape, BF16),
            pltpu.VMEM(gw.shape[1:], BF16), pltpu.VMEM(uw.shape[1:], BF16), pltpu.VMEM(dw.shape[1:], BF16),
            pltpu.VMEM((parts, rows, own), BF16), pltpu.VMEM((parts, rows, own), BF16),
            pltpu.VMEM((rows, own), F32),
            pltpu.VMEM((rows if slots == rows else total, own), BF16),
            pltpu.VMEM((parts, total, own), BF16), pltpu.VMEM((parts, total, own), BF16),
            block, block, block, block, block, block,
            pltpu.VMEM((rows, total), F32),
            dma((9,)), dma((parts,)), dma((parts,)), dma,
        ] + [dma((n,))] * 16,
        compiler_params=pltpu.CompilerParams(collective_id=1, has_side_effects=True, vmem_limit_bytes=67_000_000),
        name="experts",
    )(mixed, tokens, gain, routes, chosen, ow, gw, uw, dw)


def shards(
    tokens, previous, first_norm_gain, token_shift_share, receptance_weight, key_weight, value_weight,
    decay_down_map, decay_up_map, decay_offset, strength_down_map, strength_up_map, removal_key_scale,
    key_damping, self_term_weight, head_norm_gain, output_weight, state, second_norm_gain, routes,
    chosen_expert_weight, expert_gate_weight, expert_up_weight, expert_down_weight,
):
    parts = lax.axis_size("tp")
    n = lax.axis_size("ep")
    heads, width = state.shape[1], state.shape[2]

    def flat(values):
        return values.reshape(1, -1)

    wv, dec, ra, bl, v, rv, sv = project(
        tokens, previous, flat(first_norm_gain), token_shift_share, flat(decay_offset),
        flat(removal_key_scale), flat(key_damping), self_term_weight,
        receptance_weight, key_weight, value_weight, decay_down_map, strength_down_map,
        decay_up_map, strength_up_map, heads, width, parts,
    )
    new_state, mixed = update_state(state, wv, dec, ra, bl, v, rv, sv, flat(head_norm_gain))

    sequences, choices = routes.shape
    capacity = max(2, 3 * sequences * choices // (2 * n))
    slots = min(sequences, -(-capacity // 16) * 16)
    layer_out = experts_stage(
        mixed, tokens, flat(second_norm_gain), routes.T, chosen_expert_weight.T,
        output_weight, expert_gate_weight, expert_up_weight, expert_down_weight, n, slots, parts,
    )
    return (layer_out, new_state)


def solution(mesh):
    in_specs = (
        P("ep", "tp"), P("ep", "tp"), P(), P(), P(None, "tp"), P(None, "tp"), P(None, "tp"), P(), P(),
        P("tp"), P(), P(), P("tp"), P("tp"), P("tp", None), P("tp"), P("tp", None),
        P("ep", "tp", None, None), P(), P("ep", None), P("ep", None),
        P("ep", None, "tp"), P("ep", None, "tp"), P("ep", "tp", None),
    )
    out_specs = (P("ep", "tp"), P("ep", "tp", None, None))
    return jax.shard_map(shards, mesh=mesh, in_specs=in_specs, out_specs=out_specs, check_vma=False)
```

time: 69.5 us -> 60.1 us (0.86)
  local copies, waits for them, and re-layouts: 16.5 us -> 1.38 us
  Pallas kernels: 51.5 us -> 57.8 us
    unnamed x49 -> x1, local copies, waits for them, and re-layouts: 15 us -> 1.38 us
    pallas_call x1, Pallas kernels: 37.8 us -> 40.5 us  [experts_stage(): pl.pallas_call(expert_kernel, out_shape=jax.ShapeDtypeStruct((rows, own),...]
    pallas_call x1, Pallas kernels: 9.06 us -> 11.2 us  [project(): pl.pallas_call(project_kernel, out_shape=[jax.ShapeDtypeStruct((heads, ro...]
    pallas_call x1, Pallas kernels: 4.62 us -> 6.08 us  [update_state(): pl.pallas_call(state_kernel, grid=(seqs // rows,), out_shape=[jax.ShapeDt...]
    reshape x2 -> x0, local copies, waits for them, and re-layouts: 0.87 us -> none  [the longest x1 0.77 us: flat(): return values.reshape(1, -1)]
where the time goes in v2:
time: 60.1 us; the launch traced here: 59.8 us
  Pallas kernels  57.8 us (96%)
  local copies, waits for them, and re-layouts  1.38 us (2%)
  between operations  0.66 us (1%)
    pallas_call x1, Pallas kernels, experts_stage(): pl.pallas_call(expert_kernel, out_shape=jax.ShapeDtypeStruct((rows, own),...  40.5 us
    pallas_call x1, Pallas kernels, project(): pl.pallas_call(project_kernel, out_shape=[jax.ShapeDtypeStruct((heads, ro...  11.2 us
    pallas_call x1, Pallas kernels, update_state(): pl.pallas_call(state_kernel, grid=(seqs // rows,), out_shape=[jax.ShapeDt...  6.08 us
    unnamed x1, local copies, waits for them, and re-layouts  1.38 us

profile of v2, /device:TPU:0, one launch (start us, length us, event | category | flops | bytes accessed | tf_op | source)
XLA Modules:
  0.0 59.8 jit_solution(2117283711585186195)
XLA Ops:
  0.6 11.2 %gather_project.1 = (f32[4,32,128]{2,1,0:T(8,128)}, f32[4,32,64]{2,1,0:T(8,128)}, f32[4,32,64]{2,1,0:T(8,128)}, f32[4,32,64]{2,1,0:T(8,128)}, f32[4,32,64]{2,1,0...) custom-call(bf16[32,512]{1,0:T(8,128)(2,1)} %tokens_in.1, bf16[32,512]{1,0:T(8,128)(2,1)} %previous.1, ...), custom_call_target="tpu_custom_call" | custom-call | tf_op jit(solution)/shard_map/gather_project/pallas_call | solution.py:123
  11.8 6.1 %state_update.1 = (f32[32,4,64,64]{3,2,1,0:T(8,128)}, f32[32,256]{1,0:T(8,128)}) custom-call(f32[32,4,64,64]{3,2,1,0:T(8,128)} %state.1, f32[4,32,128]{2,1,0:T(8,128)} %get-tuple-element.11.wv, f32[4,32,64]{2,1,0:T(8,128)} %get-tuple-element.12.dec, f32[4,32,64]{2,1,0:T(8,128)} %get-tuple-element.13.ra, f32[4,32,64]{2,1,0:T(8,128)} %get-tuple-element.14.bl, ...), custom_call_target="tpu_custom_call" | custom-call | tf_op jit(solution)/shard_map/state_update/pallas_call | solution.py:183
  17.9 40.5 %experts.1 = bf16[32,512]{1,0:T(8,128)(2,1)} custom-call(f32[32,256]{1,0:T(8,128)} %get-tuple-element.18.mixed_in, bf16[32,512]{1,0:T(8,128)(2,1)} %tokens_in.1, f32[1,2048]{1,0:T(1,128)} %bitcast.9, s32[4,32]{1,0:T(4,128)} %bitcast.10, f32[4,32]{1,0:T(4,128)} %bitcast.11, bf16[256,2048]{1,0:T(8,128)(2,1)} %ow_in.1, bf16[1,2048,256]{2,1,0:T(8,128)(2,1)} %gw.1, ...), custom_call_target="tpu_custom_call" | custom-call | tf_op jit(solution)/shard_map/experts/pallas_call | solution.py:444
  58.4 1.4 %copy.27 = bf16[32,512]{1,0:T(8,128)(2,1)} copy(bf16[32,512]{1,0:T(8,128)(2,1)} %experts.1) | data formatting | bytes 65536
